TPU v7x, 32 devices: a whole 2x2x4 slice. The times are simulated.
32 devices in a mesh: ep: 8 (over z, x), tp: 4 (over y, core).
Axes of the slice: x: 2, y: 2, z: 4, core: 2. Of those that a mesh axis runs over, the one named last changes fastest.
Arguments:
- queries: bfloat16 [2048, 2, 1024], P('ep', None, 'tp')
- keys: bfloat16 [2048, 2, 256], P('ep', None, 'tp')
- values: bfloat16 [2048, 2, 256], P('ep', None, 'tp'), may hold values from -6 to 6
- query_gain: float32 [64], replicated, may hold values from 1.2 to 6
- key_gain: float32 [64], replicated, may hold values from 1.2 to 6
- out_weight: bfloat16 [1024, 2048], P('tp'), may hold values from -0.75 to 0.75
- moe_tokens: bfloat16 [4096, 2048], P(('ep', 'tp')), may hold values from -6 to 6
- moe_gain: float32 [2048], replicated, may hold values from 0.1 to 1.9
- routes: int32 [4096, 2], P(('ep', 'tp')), may hold values from 0 to 7, all different within a row; in each aligned block of 128 rows (0 to 127, 128 to 255, ...) at most 48 rows name the same one
- route_weight: float32 [4096, 2], P(('ep', 'tp')), may hold values from 0.1 to 1
- w_gate: bfloat16 [8, 2048, 1024], P('ep', None, 'tp'), may hold values from -0.125 to 0.125
- w_up: bfloat16 [8, 2048, 1024], P('ep', None, 'tp'), may hold values from -0.125 to 0.125
- w_down: bfloat16 [8, 1024, 2048], P('ep', 'tp'), may hold values from -0.1875 to 0.1875
Outputs:
- attended: bfloat16 [2048, 2, 2048], P(('ep', 'tp'))
- routed: bfloat16 [4096, 2048], P(('ep', 'tp'))
Inputs may be any that keep to these rules, and one draw needn't show every extreme that they name: `routes`: each row names 2 different experts. The rows of one device name no expert more than 48 times, and in every draw some device's rows name one expert exactly 48 times.
All inputs are finite; a program needn't handle non-finite values.
Results may differ from a plain program's by a relative error of at most 0.013.
The roundings to bfloat16 on the way count: a program that leaves them out, or rounds other values in their place, can miss the bound.
Values may be sent and summed in bfloat16 or wider, within the bound.
A program may use at most 128 MiB of HBM per device.

v0:
```python
import math
import jax
import jax.numpy as jnp
from jax import lax
from jax.sharding import PartitionSpec as P

HEAD_DIM = 64
GRID_W = 64
EPS = 1e-06
THETA = 10000.0


def turn(normed, positions):
    quarter = normed.shape[-1] // 4
    inverse = THETA ** (-jnp.arange(quarter, dtype=jnp.float32) / quarter)
    grid_row = (positions // GRID_W).astype(jnp.float32)
    grid_col = (positions % GRID_W).astype(jnp.float32)
    angles = jnp.stack([grid_row[:, None] * inverse, grid_col[:, None] * inverse], axis=1)
    cosine = jnp.cos(angles)[:, None, None]
    sine = jnp.sin(angles)[:, None, None]
    parts = normed.reshape(normed.shape[:-1] + (2, 2, quarter))
    first = parts[..., 0, :]
    second = parts[..., 1, :]
    turned = jnp.stack([first * cosine - second * sine, second * cosine + first * sine], axis=-2)
    return turned.reshape(normed.shape)


def prepare(data, positions, gain):
    heads = data.astype(jnp.float32).reshape(data.shape[0], data.shape[1], -1, HEAD_DIM)
    normed = heads * lax.rsqrt(jnp.mean(heads * heads, axis=-1, keepdims=True) + EPS) * gain
    return turn(normed, positions).astype(jnp.bfloat16)


def per_device(
    queries,
    keys,
    values,
    query_gain,
    key_gain,
    out_weight,
    moe_tokens,
    moe_gain,
    routes,
    route_weight,
    w_gate,
    w_up,
    w_down,
):
    pos_count = queries.shape[0]
    seq_count = queries.shape[1]
    positions = lax.axis_index("ep") * pos_count + jnp.arange(pos_count, dtype=jnp.int32)
    q_rot = prepare(queries, positions, query_gain)
    k_rot = prepare(keys, positions, key_gain)
    kv_local = k_rot.shape[2]
    groups = q_rot.shape[2] // kv_local
    value_heads = values.reshape(pos_count, seq_count, kv_local, HEAD_DIM)
    q_group = q_rot.reshape(pos_count, seq_count, kv_local, groups, HEAD_DIM)
    scale = HEAD_DIM ** (-0.5)
    start_state = (
        jnp.full((seq_count, kv_local, groups, pos_count), -1e30, jnp.float32),
        jnp.zeros((seq_count, kv_local, groups, pos_count), jnp.float32),
        jnp.zeros((pos_count, seq_count, kv_local, groups, HEAD_DIM), jnp.float32),
    )
    carry = start_state
    key_piece = lax.all_gather(k_rot, "ep", axis=0, tiled=True)
    value_piece = lax.all_gather(value_heads, "ep", axis=0, tiled=True)
    count = key_piece.shape[0]
    width = math.gcd(count, 512)
    key_split = key_piece.reshape(count // width, width, seq_count, kv_local, HEAD_DIM)
    value_split = value_piece.reshape(count // width, width, seq_count, kv_local, HEAD_DIM)

    def step(state, block):
        best, total, accum = state
        key_block, value_block = block
        scores = (
            jnp.einsum("pskgd,lskd->skgpl", q_group, key_block, preferred_element_type=jnp.float32)
            * scale
        )
        new_best = jnp.maximum(best, jnp.max(scores, axis=-1))
        factor = jnp.exp(best - new_best)
        expo = jnp.exp(scores - new_best[..., None])
        total = total * factor + jnp.sum(expo, axis=-1)
        added = jnp.einsum(
            "skgpl,lskd->pskgd",
            expo.astype(jnp.bfloat16),
            value_block,
            preferred_element_type=jnp.float32,
        )
        accum = accum * jnp.transpose(factor, (3, 0, 1, 2))[..., None] + added
        return ((new_best, total, accum), None)

    carry, _ = lax.scan(step, carry, (key_split, value_split))
    best, total, accum = carry
    mixed = (accum / jnp.transpose(total, (3, 0, 1, 2))[..., None]).astype(jnp.bfloat16)
    mixed = mixed.reshape(pos_count, seq_count, -1)
    rows = mixed
    product = jnp.dot(
        rows.reshape(pos_count // lax.axis_size("tp") * lax.axis_size("tp") * seq_count, -1),
        out_weight,
        preferred_element_type=jnp.float32,
    )
    attended = lax.psum_scatter(
        product.reshape(
            pos_count // lax.axis_size("tp") * lax.axis_size("tp"), seq_count, -1
        ).astype(jnp.bfloat16),
        "tp",
        scatter_dimension=0,
        tiled=True,
    )
    tok_count = moe_tokens.shape[0]
    top_count = routes.shape[1]
    experts = lax.axis_size("ep")
    capacity = max(2, (3 * tok_count * top_count + 2 * experts - 1) // (2 * experts))
    token_float = moe_tokens.astype(jnp.float32)
    normed = (
        token_float
        * lax.rsqrt(jnp.mean(token_float * token_float, axis=-1, keepdims=True) + EPS)
        * moe_gain
    ).astype(jnp.bfloat16)
    hits = (routes[:, :, None] == jnp.arange(experts, dtype=jnp.int32)[None, None, :]).astype(
        jnp.float32
    )
    pair_count = tok_count * top_count
    flat_hits = hits.reshape(pair_count, experts)
    pair_index = jnp.arange(pair_count, dtype=jnp.int32)
    earlier = (pair_index[:, None] > pair_index[None, :]).astype(jnp.float32)
    before = jnp.dot(earlier, flat_hits, precision=lax.Precision.HIGHEST)
    rank = jnp.sum(before * flat_hits, axis=-1).astype(jnp.int32).reshape(tok_count, top_count)
    slot = routes * capacity + rank
    table = jnp.arange(experts * capacity, dtype=jnp.int32)
    dispatch = jnp.sum(
        (slot[None, :, :] == table[:, None, None]).astype(jnp.float32), axis=2
    ).astype(jnp.bfloat16)
    send = jnp.dot(dispatch, normed, preferred_element_type=jnp.float32).astype(jnp.bfloat16)
    received = lax.all_to_all(send, "ep", split_axis=0, concat_axis=0, tiled=True)
    rows = lax.all_gather(received, "tp", axis=0, tiled=True)
    gate = jnp.dot(rows, w_gate[0], preferred_element_type=jnp.float32)
    up = jnp.dot(rows, w_up[0], preferred_element_type=jnp.float32)
    hidden = (jax.nn.silu(gate) * up).astype(jnp.bfloat16)
    rows = hidden
    result = lax.psum_scatter(
        jnp.dot(rows, w_down[0], preferred_element_type=jnp.float32).astype(jnp.bfloat16),
        "tp",
        scatter_dimension=0,
        tiled=True,
    )
    returned_rows = lax.all_to_all(result, "ep", split_axis=0, concat_axis=0, tiled=True)
    combined = jnp.zeros((tok_count, returned_rows.shape[-1]), jnp.float32)
    for choice_index in range(top_count):
        picker = (slot[:, choice_index : choice_index + 1] == table[None, :]).astype(jnp.bfloat16)
        picked = jnp.dot(picker, returned_rows, preferred_element_type=jnp.float32)
        combined = combined + picked * route_weight[:, choice_index : choice_index + 1]
    return (attended, combined.astype(jnp.bfloat16))


def solution(mesh):
    in_specs = (
        P("ep", None, "tp"),
        P("ep", None, "tp"),
        P("ep", None, "tp"),
        P(),
        P(),
        P("tp", None),
        P(("ep", "tp"), None),
        P(),
        P(("ep", "tp"), None),
        P(("ep", "tp"), None),
        P("ep", None, "tp"),
        P("ep", None, "tp"),
        P("ep", "tp", None),
    )
    out_specs = (P(("ep", "tp"), None, None), P(("ep", "tp"), None))
    return jax.shard_map(
        per_device, mesh=mesh, in_specs=in_specs, out_specs=out_specs, check_vma=False
    )
```

profile of v0, /device:TPU:0, one launch (start us, length us, event | category | flops | bytes accessed | tf_op | source)
XLA Modules:
  0.0 241.3 jit_solution(14699746552922616163)
XLA Ops:
  7.2 0.0 copy-start
  7.2 0.0 copy-start.7
  7.2 0.0 all-gather.3.cloned.1.call-start
  7.2 1.4 fusion.28
  8.6 0.8 copy.53
  9.4 0.1 eq.63
  9.5 0.2 fusion.27
  9.8 0.1 convert_element_type.99
  9.9 0.1 copy.54
  10.0 0.7 multiply_add_fusion
  10.7 0.1 convert_reduce_fusion
  10.7 1.7 convolution_convert_fusion.2
  12.4 44.2 %all_to_all.24 = bf16[8,48,2048]{2,1,0:T(8,128)(2,1)} all-to-all(bf16[8,48,2048]{2,1,0:T(8,128)(2,1)S(1)} %bitcast.136), channel_id=1, replica_groups=mesh['ep'=8,'tp'=4] {'ep'}, dimensions={0} | all-to-all | bytes 3145728 | tf_op jit(solution)/shard_map/all_to_all | solution.py:135
  56.6 0.0 all-gather.3.cloned.1.call-update
  56.6 0.0 copy-start.8
  56.7 0.0 reduce-scatter.5.cloned.1.call-start
  56.7 45.5 %all-gather.3.cloned.1.call-done = bf16[1536,2048]{1,0:T(8,128)(2,1)} async-done(((bf16[384,2048]{1,0:T(8,128)(2,1)}), bf16[1536,2048]{1,0:T(8,128)(2,1)}) %all-gather.3.cloned.1.call-update) | async-done | bytes 6291472 | tf_op jit(solution)/shard_map/all_gather | solution.py:136
  102.2 0.0 copy-done.7
  102.2 5.8 %fusion.34 = f32[1536,256]{1,0:T(8,128)} fusion(bf16[1536,2048]{1,0:T(8,128)(2,1)} %all-gather.3.cloned.1.call-done, bf16[1,2048,256]{2,1,0:T(8,128)(2,1)S(1)} %copy-done.7), kind=kOutput, calls=%fused_computation.44 | convolution fusion | flops 1610612736 | bytes 8912896 | tf_op jit(solution)/shard_map/dot_general | solution.py:137
  108.0 0.0 copy-done
  108.0 0.0 copy-done.8
  108.0 12.3 %convolution_convert_fusion = bf16[1536,2048]{1,0:T(8,128)(2,1)} fusion(bf16[1536,2048]{1,0:T(8,128)(2,1)} %all-gather.3.cloned.1.call-done, f32[1536,256]{1,0:T(8,128)} %fusion.34, bf16[1,256,2048]{2,1,0:T(8,128)(2,1)S(1)} %copy-done, bf16[1,2048,256]{2,1,0:T(8,128)(2,1)S(1)} %copy-done.8), kind=kOutput, calls=%fused_computation.26 | convolution fusion | flops 3226730496 | bytes 16252928 | tf_op jit(solution)/shard_map/dot_general | solution.py:142
  120.3 0.0 copy-start.3
  120.3 0.0 reduce-scatter.5.cloned.1.call-update
  120.3 0.0 reduce-scatter.3.cloned.1.call-start
  120.4 0.5 copy-done.6
  120.9 0.1 mul.275
  121.0 0.2 copy-done.2
  121.3 0.2 copy.49
  121.5 0.1 broadcast_multiply_fusion.1
  121.5 0.1 fusion.47
  121.7 0.1 fusion.42
  121.9 31.5 %all_gather.9 = bf16[2048,2,1,64]{0,3,1,2:T(8,128)(2,1)S(1)} all-gather(bf16[256,2,1,64]{0,3,1,2:T(8,128)(2,1)S(1)} %bitcast.146), channel_id=1, replica_groups=mesh['ep'=8,'tp'=4] {'ep'}, dimensions={0}, use_global_device_ids=true | all-gather | bytes 589824 | tf_op jit(solution)/shard_map/all_gather | solution.py:65
  153.4 0.0 copy-done.3
  153.4 31.5 %all-gather = bf16[2048,2,64]{0,2,1:T(8,128)(2,1)S(1)} all-gather(bf16[256,2,64]{0,2,1:T(8,128)(2,1)S(1)} %copy-done.3), channel_id=2, replica_groups=mesh['ep'=8,'tp'=4] {'ep'}, dimensions={0}, use_global_device_ids=true | all-gather | bytes 589824 | tf_op jit(solution)/shard_map/all_gather | solution.py:66
  184.9 0.4 reshape.289
  185.2 0.1 copy.51
  185.3 0.1 bitcast_reduce_fusion.1
  185.4 0.1 multiply_multiply_fusion
  185.5 0.1 subtract_convert_fusion
  185.7 10.0 %while.15 = (s32[]{:T(128)}, f32[2,1,4,256]{3,2,0,1:T(4,128)S(1)}, f32[2,1,4,256]{3,2,0,1:T(4,128)S(1)}, f32[256,2,1,4,64]{0,4,3,1,2:T(8,128)S(1)}, bf16[4,512,2...) while((s32[]{:T(128)}, f32[2,1,4,256]{3,2,0,1:T(4,128)S(1)}, ...), condition=%wide.region_5.6_spmd.clone, body=%wide.region_2.5_spmd.clone.sunk | while | flops 277229568 | bytes 14286969 | solution.py:92
  185.7 0.8 bitcast_reduce_fusion.3
  186.5 0.7 fusion.67
  187.2 0.9 fusion.68
  188.2 0.8 bitcast_reduce_fusion.3
  189.0 0.7 fusion.67
  189.7 0.9 fusion.68
  190.7 0.8 bitcast_reduce_fusion.3
  191.5 0.7 fusion.67
  192.2 0.9 fusion.68
  193.2 0.8 bitcast_reduce_fusion.3
  194.0 0.7 fusion.67
  194.7 0.9 fusion.68
  195.7 0.0 copy-start.4
  195.8 3.3 %convolution_convert_fusion.1 = bf16[256,2,2048]{2,0,1:T(8,128)(2,1)} fusion(bf16[256,2,256]{0,2,1:T(8,128)(2,1)S(1)} %bitcast.143, bf16[256,2048]{1,0:T(8,128)(2,1)} %param.20), kind=kOutput, calls=%fused_computation.27 | convolution fusion | flops 537919488 | bytes 3407872 | tf_op jit(solution)/shard_map/dot_general | solution.py:97
  199.1 0.0 reduce-scatter.3.cloned.1.call-update
  199.1 0.0 reduce-scatter.5.cloned.1.call-done
  199.1 5.7 %all-to-all-start.1 = ((bf16[8,48,2048]{2,1,0:T(8,128)(2,1)}), bf16[8,48,2048]{2,1,0:T(8,128)(2,1)S(1)}, u32[]{:S(2)}, u32[]{:S(2)}) async-start(bf16[8,48,2048]{2,1,0:T(8,128)(2,1)} %bitcast.142), calls=%async_computation.3 | async-start | bytes 3145728 | tf_op jit(solution)/shard_map/all_to_all | solution.py:147
  204.8 0.0 copy-done.4
  204.8 25.8 %reduce-scatter.3.cloned.1.call-done = bf16[64,2,2048]{2,0,1:T(8,128)(2,1)} async-done(((bf16[256,2,2048]{2,0,1:T(8,128)(2,1)}), bf16[64,2,2048]{2,0,1:T(8,128)(2,1)}) %reduce-scatter.3.cloned.1.call-update) | async-done | bytes 524304 | tf_op jit(solution)/shard_map/reduce_scatter | solution.py:102
  230.6 2.4 copy.55
  232.9 0.0 all-to-all-done.1
  232.9 0.5 convolution_multiply_fusion.2
  233.4 1.3 fusion.26
  (35 shorter events, 0.4 us)
Async XLA Ops:
  7.2 100.8 %copy-start = (bf16[1,256,2048]{2,1,0:T(8,128)(2,1)S(1)}, bf16[1,256,2048]{2,1,0:T(8,128)(2,1)}, u32[]{:S(2)}) copy-start(bf16[1,256,2048]{2,1,0:T(8,128)(2,1)} %param.27) | copy-start | bytes 3145732
  7.2 95.0 %copy-start.7 = (bf16[1,2048,256]{2,1,0:T(8,128)(2,1)S(1)}, bf16[1,2048,256]{2,1,0:T(8,128)(2,1)}, u32[]{:S(2)}) copy-start(bf16[1,2048,256]{2,1,0:T(8,128)(2,1)} %param.25) | copy-start | bytes 3145732
  7.2 95.0 %all-gather.3.cloned.1.call-start = ((), (), s32[]{:S(2)}) async-start(), calls=%async_computation.5 | async-start | bytes 7864320 | tf_op jit(solution)/shard_map/all_gather | solution.py:136
  56.6 51.4 %copy-start.8 = (bf16[1,2048,256]{2,1,0:T(8,128)(2,1)S(1)}, bf16[1,2048,256]{2,1,0:T(8,128)(2,1)}, u32[]{:S(2)}) copy-start(bf16[1,2048,256]{2,1,0:T(8,128)(2,1)} %param.26) | copy-start | bytes 3145732
  56.7 142.5 %reduce-scatter.5.cloned.1.call-start = ((), (), s32[]{:S(2)}) async-start(), calls=%async_computation.6 | async-start | bytes 7864320 | tf_op jit(solution)/shard_map/reduce_scatter | solution.py:141
  120.3 0.7 copy-start.6
  120.3 1.0 copy-start.2
  120.3 1.4 copy-start.1
  120.3 1.4 copy-start.5
  120.3 33.1 %copy-start.3 = (bf16[256,2,64]{0,2,1:T(8,128)(2,1)S(1)}, bf16[256,2,64]{0,2,1:T(8,128)(2,1)}, u32[]{:S(2)}) copy-start(bf16[256,2,64]{0,2,1:T(8,128)(2,1)} %param.17) | copy-start | bytes 196612
  120.3 110.2 %reduce-scatter.3.cloned.1.call-start = ((), (), s32[]{:S(2)}) async-start(), calls=%async_computation.4 | async-start | bytes 2621440 | tf_op jit(solution)/shard_map/reduce_scatter | solution.py:102
  195.7 9.0 %copy-start.4 = (f32[128,2]{0,1:T(2,128)S(1)}, f32[128,2]{0,1:T(2,128)}, u32[]{:S(2)}) copy-start(f32[128,2]{0,1:T(2,128)} %param.24) | copy-start | bytes 3076
  199.1 33.8 %all-to-all-start.1 = ((bf16[8,48,2048]{2,1,0:T(8,128)(2,1)}), bf16[8,48,2048]{2,1,0:T(8,128)(2,1)S(1)}, u32[]{:S(2)}, u32[]{:S(2)}) async-start(bf16[8,48,2048]{2,1,0:T(8,128)(2,1)} %bitcast.142), calls=%async_computation.3 | async-start | bytes 3145728 | tf_op jit(solution)/shard_map/all_to_all | solution.py:147
Sparse Core Ops, SparseCore 0:
  56.8 45.3 all-gather.2
  120.5 58.8 reduce-scatter.4
  199.2 31.3 reduce-scatter.2
where the time goes:
time: 242 us; the launch traced here: 241 us
  blocking collectives  107 us (44%)
  waiting for transfers between devices  71.3 us (29%)
  matrix products  31.9 us (13%)
  between operations  14 us (6%)
  other arithmetic  5.82 us (2%)
  starting transfers between devices  5.78 us (2%)
  local copies, waits for them, and re-layouts  5.07 us (2%)
    all_gather x1, waiting for transfers between devices, per_device(): rows = lax.all_gather(received, 'tp', axis=0, tiled=True)  45.5 us
    all_to_all x1, blocking collectives, per_device(): lax.all_to_all(send, 'ep', split_axis=0, concat_axis=0, tiled=True)  44.2 us
    all_gather x1, blocking collectives, per_device(): value_piece = lax.all_gather(value_heads, 'ep', axis=0, tiled=True)  31.5 us
    all_gather x1, blocking collectives, per_device(): key_piece = lax.all_gather(k_rot, 'ep', axis=0, tiled=True)  31.5 us
    reduce_scatter x1, waiting for transfers between devices, per_device(): lax.psum_scatter(product.reshape(pos_count // lax.axis_size('tp') * lax.a...  25.8 us
    dot_general x1, matrix products, per_device(): jnp.dot(rows, w_down[0], preferred_element_type=jnp.float32)  12.3 us
    dot_general x1, matrix products, per_device(): gate = jnp.dot(rows, w_gate[0], preferred_element_type=jnp.float32)  5.8 us
    all_to_all x1, starting transfers between devices, per_device(): lax.all_to_all(result, 'ep', split_axis=0, concat_axis=0, tiled=True)  5.66 us
  transfers between devices with their start and end apart: 4, of which 2 were waited for; matrix products, arithmetic and copies ran while one was open for 7% of the time, Pallas kernels for 0%

commit v1 on v0

--- a/solution.py
+++ b/solution.py
@@ -63,7 +63,12 @@
     )
     carry = start_state
     key_piece = lax.all_gather(k_rot, "ep", axis=0, tiled=True)
-    value_piece = lax.all_gather(value_heads, "ep", axis=0, tiled=True)
+    ring = [value_heads]
+    for hop in range(7):
+        ring.append(lax.ppermute(ring[-1], "ep", [(dev, (dev + 1) % 8) for dev in range(8)]))
+    value_piece = jnp.roll(
+        jnp.concatenate(ring[::-1], axis=0), (lax.axis_index("ep") + 1) * ring[0].shape[0], axis=0
+    )
     count = key_piece.shape[0]
     width = math.gcd(count, 512)
     key_split = key_piece.reshape(count // width, width, seq_count, kv_local, HEAD_DIM)

time: 242 us -> 249 us (1.029)
  waiting for transfers between devices: 71.3 us -> 108 us
  blocking collectives: 107 us -> 75.8 us
    ppermute x0 -> x7, waiting for transfers between devices: none -> 37.7 us  [per_device(): lax.ppermute(ring[-1], 'ep', [(dev, (dev + 1) % 8) for dev in range(8)])]
    all_gather x1 -> x0, blocking collectives: 31.5 us -> none  [per_device(): value_piece = lax.all_gather(value_heads, 'ep', axis=0, tiled=True)]
    ppermute x0 -> x7, starting transfers between devices: none -> 3.55 us  [per_device(): lax.ppermute(ring[-1], 'ep', [(dev, (dev + 1) % 8) for dev in range(8)])]
  transfers between devices with their start and end apart: 4 -> 11, of which waited for: 2 -> 8; matrix products, arithmetic and copies ran while one was open for 7% -> 7% of each run, Pallas kernels for 0% -> 0%
where the time goes in v1:
time: 249 us; the launch traced here: 248 us
  waiting for transfers between devices  108 us (43%)
  blocking collectives  75.8 us (30%)
  matrix products  31.9 us (13%)
  between operations  14.1 us (6%)
  starting transfers between devices  7.27 us (3%)
  other arithmetic  5.81 us (2%)
  local copies, waits for them, and re-layouts  4.8 us (2%)
    all_gather x1, waiting for transfers between devices, per_device(): rows = lax.all_gather(received, 'tp', axis=0, tiled=True)  45.5 us
    all_to_all x1, blocking collectives, per_device(): lax.all_to_all(send, 'ep', split_axis=0, concat_axis=0, tiled=True)  44.2 us
    ppermute x7, waiting for transfers between devices, per_device(): lax.ppermute(ring[-1], 'ep', [(dev, (dev + 1) % 8) for dev in range(8)])  37.7 us
    all_gather x1, blocking collectives, per_device(): key_piece = lax.all_gather(k_rot, 'ep', axis=0, tiled=True)  31.6 us
    reduce_scatter x1, waiting for transfers between devices, per_device(): lax.psum_scatter(product.reshape(pos_count // lax.axis_size('tp') * lax.a...  25.2 us
    dot_general x1, matrix products, per_device(): jnp.dot(rows, w_down[0], preferred_element_type=jnp.float32)  12.3 us
    dot_general x1, matrix products, per_device(): gate = jnp.dot(rows, w_gate[0], preferred_element_type=jnp.float32)  5.76 us
  transfers between devices with their start and end apart: 11, of which 8 were waited for; matrix products, arithmetic and copies ran while one was open for 7% of the time, Pallas kernels for 0%

profile of v1, /device:TPU:0, one launch (start us, length us, event | category | flops | bytes accessed | tf_op | source)
XLA Modules:
  0.0 248.3 jit_solution(2624585522900132535)
XLA Ops:
  7.2 0.0 copy-start
  7.2 0.0 all-gather.2.cloned.1.call-start
  7.2 1.4 fusion.28
  8.6 0.8 copy.53
  9.4 0.1 eq.66
  9.5 0.2 fusion.27
  9.8 0.1 convert_element_type.99
  9.9 0.1 copy.54
  10.0 0.7 multiply_add_fusion
  10.7 0.1 convert_reduce_fusion
  10.7 1.7 convolution_convert_fusion.2
  12.4 44.2 %all_to_all.24 = bf16[8,48,2048]{2,1,0:T(8,128)(2,1)} all-to-all(bf16[8,48,2048]{2,1,0:T(8,128)(2,1)S(1)} %bitcast.141), channel_id=1, replica_groups=mesh['ep'=8,'tp'=4] {'ep'}, dimensions={0} | all-to-all | bytes 3145728 | tf_op jit(solution)/shard_map/all_to_all | solution.py:140
  56.6 0.0 all-gather.2.cloned.1.call-update
  56.6 0.0 copy-start.8
  56.7 0.0 reduce-scatter.5.cloned.1.call-start
  56.7 45.5 %all-gather.2.cloned.1.call-done = bf16[1536,2048]{1,0:T(8,128)(2,1)} async-done(((bf16[384,2048]{1,0:T(8,128)(2,1)}), bf16[1536,2048]{1,0:T(8,128)(2,1)}) %all-gather.2.cloned.1.call-update) | async-done | bytes 6291472 | tf_op jit(solution)/shard_map/all_gather | solution.py:141
  102.2 5.8 %fusion.34 = f32[1536,256]{1,0:T(8,128)} fusion(bf16[1536,2048]{1,0:T(8,128)(2,1)} %all-gather.2.cloned.1.call-done, bf16[1,2048,256]{2,1,0:T(8,128)(2,1)S(1)} %copy-done.7), kind=kOutput, calls=%fused_computation.44 | convolution fusion | flops 1610612736 | bytes 8912896 | tf_op jit(solution)/shard_map/dot_general | solution.py:142
  108.0 12.3 %convolution_convert_fusion = bf16[1536,2048]{1,0:T(8,128)(2,1)} fusion(bf16[1536,2048]{1,0:T(8,128)(2,1)} %all-gather.2.cloned.1.call-done, f32[1536,256]{1,0:T(8,128)} %fusion.34, bf16[1,256,2048]{2,1,0:T(8,128)(2,1)S(1)} %copy-done, bf16[1,2048,256]{2,1,0:T(8,128)(2,1)S(1)} %copy-done.8), kind=kOutput, calls=%fused_computation.26 | convolution fusion | flops 3226730496 | bytes 16252928 | tf_op jit(solution)/shard_map/dot_general | solution.py:147
  120.3 0.0 copy-start.5
  120.3 0.0 reduce-scatter.5.cloned.1.call-update
  120.3 0.0 reduce-scatter.3.cloned.1.call-start
  120.4 0.7 copy-done.3
  121.1 1.5 collective-permute-start
  122.6 0.1 mul.278
  122.7 0.2 copy.49
  122.9 0.1 broadcast_multiply_fusion.1
  123.0 0.1 fusion.47
  123.1 0.1 bitcast_reduce_fusion.1
  123.2 0.1 multiply_multiply_fusion
  123.3 0.1 subtract_convert_fusion
  123.4 4.6 %collective-permute-done = bf16[256,2,1,64]{0,3,1,2:T(8,128)(2,1)S(1)} collective-permute-done((bf16[256,2,1,64]{0,3,1,2:T(8,128)(2,1)S(1)}, bf16[256,2,1,64]{0,3,1,2:T(8,128)(2,1)S(1)}, u32[]{:S(2)}, u32[]{:S(2)}) %collective-permute-start) | collective-permute-done | bytes 65568 | tf_op jit(solution)/shard_map/ppermute | solution.py:68
  128.1 7.0 %collective-permute-done.1 = bf16[256,2,1,64]{0,3,1,2:T(8,128)(2,1)S(1)} collective-permute-done((bf16[256,2,1,64]{0,3,1,2:T(8,128)(2,1)S(1)}, bf16[256,2,1,64]{0,3,1,2:T(8,128)(2,1)S(1)}, u32[]{:S(2)}, u32[]{:S(2)}) %collective-permute-start.1) | collective-permute-done | bytes 65568 | tf_op jit(solution)/shard_map/ppermute | solution.py:68
  135.0 0.1 fusion.42
  135.1 6.9 %collective-permute-done.2 = bf16[256,2,1,64]{0,3,1,2:T(8,128)(2,1)S(1)} collective-permute-done((bf16[256,2,1,64]{0,3,1,2:T(8,128)(2,1)S(1)}, bf16[256,2,1,64]{0,3,1,2:T(8,128)(2,1)S(1)}, u32[]{:S(2)}, u32[]{:S(2)}) %collective-permute-start.2) | collective-permute-done | bytes 65568 | tf_op jit(solution)/shard_map/ppermute | solution.py:68
  142.0 6.9 %collective-permute-done.3 = bf16[256,2,1,64]{0,3,1,2:T(8,128)(2,1)S(1)} collective-permute-done((bf16[256,2,1,64]{0,3,1,2:T(8,128)(2,1)S(1)}, bf16[256,2,1,64]{0,3,1,2:T(8,128)(2,1)S(1)}, u32[]{:S(2)}, u32[]{:S(2)}) %collective-permute-start.3) | collective-permute-done | bytes 65568 | tf_op jit(solution)/shard_map/ppermute | solution.py:68
  149.0 0.0 collective-permute-start.4
  149.0 7.2 %collective-permute-done.4 = bf16[256,2,1,64]{0,3,1,2:T(8,128)(2,1)S(1)} collective-permute-done((bf16[256,2,1,64]{0,3,1,2:T(8,128)(2,1)S(1)}, bf16[256,2,1,64]{0,3,1,2:T(8,128)(2,1)S(1)}, u32[]{:S(2)}, u32[]{:S(2)}) %collective-permute-start.4) | collective-permute-done | bytes 65568 | tf_op jit(solution)/shard_map/ppermute | solution.py:68
  156.1 31.6 %all_gather.6 = bf16[2048,2,1,64]{0,3,1,2:T(8,128)(2,1)S(1)} all-gather(bf16[256,2,1,64]{0,3,1,2:T(8,128)(2,1)S(1)} %bitcast.153), channel_id=1, replica_groups=mesh['ep'=8,'tp'=4] {'ep'}, dimensions={0}, use_global_device_ids=true | all-gather | bytes 589824 | tf_op jit(solution)/shard_map/all_gather | solution.py:65
  187.8 0.0 collective-permute-done.5
  187.8 2.1 collective-permute-start.6
  189.9 5.1 %collective-permute-done.6 = bf16[256,2,1,64]{0,3,1,2:T(8,128)(2,1)S(1)} collective-permute-done((bf16[256,2,1,64]{0,3,1,2:T(8,128)(2,1)S(1)}, bf16[256,2,1,64]{0,3,1,2:T(8,128)(2,1)S(1)}, u32[]{:S(2)}, u32[]{:S(2)}) %collective-permute-start.6) | collective-permute-done | bytes 65568 | tf_op jit(solution)/shard_map/ppermute | solution.py:68
  195.2 0.1 constant_dynamic-slice_fusion
  195.3 10.0 %while.15 = (s32[]{:T(128)}, f32[2,1,4,256]{3,2,0,1:T(4,128)S(1)}, f32[2,1,4,256]{3,2,0,1:T(4,128)S(1)}, f32[256,2,1,4,64]{0,4,3,1,2:T(8,128)S(1)}, bf16[4,512,2...) while((s32[]{:T(128)}, f32[2,1,4,256]{3,2,0,1:T(4,128)S(1)}, ...), condition=%wide.region_5.6_spmd.clone, body=%wide.region_2.5_spmd.clone.sunk | while | flops 277229568 | bytes 14286969 | solution.py:97
  195.3 0.8 bitcast_reduce_fusion.3
  196.1 0.7 fusion.67
  196.8 0.9 fusion.68
  197.8 0.8 bitcast_reduce_fusion.3
  198.6 0.7 fusion.67
  199.3 0.9 fusion.68
  200.3 0.8 bitcast_reduce_fusion.3
  201.1 0.7 fusion.67
  201.8 0.9 fusion.68
  202.8 0.8 bitcast_reduce_fusion.3
  203.6 0.7 fusion.67
  204.3 1.0 fusion.68
  205.4 0.0 copy-start.4
  205.4 3.3 %convolution_convert_fusion.1 = bf16[256,2,2048]{2,0,1:T(8,128)(2,1)} fusion(bf16[256,2,256]{0,2,1:T(8,128)(2,1)S(1)} %bitcast.150, bf16[256,2048]{1,0:T(8,128)(2,1)} %param.20), kind=kOutput, calls=%fused_computation.27 | convolution fusion | flops 537919488 | bytes 3407872 | tf_op jit(solution)/shard_map/dot_general | solution.py:102
  208.7 0.0 reduce-scatter.3.cloned.1.call-update
  208.7 0.0 reduce-scatter.5.cloned.1.call-done
  208.8 3.6 %all-to-all-start.1 = ((bf16[8,48,2048]{2,1,0:T(8,128)(2,1)}), bf16[8,48,2048]{2,1,0:T(8,128)(2,1)S(1)}, u32[]{:S(2)}, u32[]{:S(2)}) async-start(bf16[8,48,2048]{2,1,0:T(8,128)(2,1)} %bitcast.149), calls=%async_computation.3 | async-start | bytes 3145728 | tf_op jit(solution)/shard_map/all_to_all | solution.py:152
  212.4 25.2 %reduce-scatter.3.cloned.1.call-done = bf16[64,2,2048]{2,0,1:T(8,128)(2,1)} async-done(((bf16[256,2,2048]{2,0,1:T(8,128)(2,1)}), bf16[64,2,2048]{2,0,1:T(8,128)(2,1)}) %reduce-scatter.3.cloned.1.call-update) | async-done | bytes 524304 | tf_op jit(solution)/shard_map/reduce_scatter | solution.py:107
  237.6 2.4 copy.55
  240.0 0.5 convolution_multiply_fusion.2
  240.5 1.3 fusion.26
  (64 shorter events, 0.6 us)
Async XLA Ops:
  7.2 100.8 %copy-start = (bf16[1,256,2048]{2,1,0:T(8,128)(2,1)S(1)}, bf16[1,256,2048]{2,1,0:T(8,128)(2,1)}, u32[]{:S(2)}) copy-start(bf16[1,256,2048]{2,1,0:T(8,128)(2,1)} %param.27) | copy-start | bytes 3145732
  7.2 95.0 %copy-start.7 = (bf16[1,2048,256]{2,1,0:T(8,128)(2,1)S(1)}, bf16[1,2048,256]{2,1,0:T(8,128)(2,1)}, u32[]{:S(2)}) copy-start(bf16[1,2048,256]{2,1,0:T(8,128)(2,1)} %param.25) | copy-start | bytes 3145732
  7.2 95.0 %all-gather.2.cloned.1.call-start = ((), (), s32[]{:S(2)}) async-start(), calls=%async_computation.5 | async-start | bytes 7864320 | tf_op jit(solution)/shard_map/all_gather | solution.py:141
  56.6 51.3 %copy-start.8 = (bf16[1,2048,256]{2,1,0:T(8,128)(2,1)S(1)}, bf16[1,2048,256]{2,1,0:T(8,128)(2,1)}, u32[]{:S(2)}) copy-start(bf16[1,2048,256]{2,1,0:T(8,128)(2,1)} %param.26) | copy-start | bytes 3145732
  56.7 152.1 %reduce-scatter.5.cloned.1.call-start = ((), (), s32[]{:S(2)}) async-start(), calls=%async_computation.6 | async-start | bytes 7864320 | tf_op jit(solution)/shard_map/reduce_scatter | solution.py:146
  120.3 0.8 copy-start.3
  120.3 2.3 copy-start.6
  120.3 2.4 copy-start.2
  120.3 3.1 %copy-start.1 = (bf16[256,2,64]{0,2,1:T(8,128)(2,1)S(1)}, bf16[256,2,64]{0,2,1:T(8,128)(2,1)}, u32[]{:S(2)}) copy-start(bf16[256,2,64]{0,2,1:T(8,128)(2,1)} %param.16) | copy-start | bytes 196612
  120.3 14.8 %copy-start.5 = (f32[64]{0:T(128)S(1)}, f32[64]{0:T(128)}, u32[]{:S(2)}) copy-start(f32[64]{0:T(128)} %param.19) | copy-start | bytes 772
  120.3 117.3 %reduce-scatter.3.cloned.1.call-start = ((), (), s32[]{:S(2)}) async-start(), calls=%async_computation.4 | async-start | bytes 2621440 | tf_op jit(solution)/shard_map/reduce_scatter | solution.py:107
  121.1 7.0 %collective-permute-start = (bf16[256,2,1,64]{0,3,1,2:T(8,128)(2,1)S(1)}, bf16[256,2,1,64]{0,3,1,2:T(8,128)(2,1)S(1)}, u32[]{:S(2)}, u32[]{:S(2)}) collective-permute-start(bf16[256,2,1,64]{0,3,1,2:T(8,128)(2,1)S(1)} %bitcast.154), channel_id=1, source_target_pairs={{0,4},{4,8},{8,12},{12,16},{16,20},{20,24},{24,28},{28,0},{1,5},{5... | collective-permute-start | bytes 196616 | tf_op jit(solution)/shard_map/ppermute | solution.py:68
  128.1 7.0 %collective-permute-start.1 = (bf16[256,2,1,64]{0,3,1,2:T(8,128)(2,1)S(1)}, bf16[256,2,1,64]{0,3,1,2:T(8,128)(2,1)S(1)}, u32[]{:S(2)}, u32[]{:S(2)}) collective-permute-start(bf16[256,2,1,64]{0,3,1,2:T(8,128)(2,1)S(1)} %collective-permute-done), channel_id=1, source_target_pairs={{0,4},{4,8},{8,12},{12,16},{16,20},{20,24},{24,28},{28,0},{1,5},{5... | collective-permute-start | bytes 196616 | tf_op jit(solution)/shard_map/ppermute | solution.py:68
  135.0 7.0 %collective-permute-start.2 = (bf16[256,2,1,64]{0,3,1,2:T(8,128)(2,1)S(1)}, bf16[256,2,1,64]{0,3,1,2:T(8,128)(2,1)S(1)}, u32[]{:S(2)}, u32[]{:S(2)}) collective-permute-start(bf16[256,2,1,64]{0,3,1,2:T(8,128)(2,1)S(1)} %collective-permute-done.1), channel_id=1, source_target_pairs={{0,4},{4,8},{8,12},{12,16},{16,20},{20,24},{24,28},{28,0},{1,5},{5... | collective-permute-start | bytes 196616 | tf_op jit(solution)/shard_map/ppermute | solution.py:68
  142.0 7.0 %collective-permute-start.3 = (bf16[256,2,1,64]{0,3,1,2:T(8,128)(2,1)S(1)}, bf16[256,2,1,64]{0,3,1,2:T(8,128)(2,1)S(1)}, u32[]{:S(2)}, u32[]{:S(2)}) collective-permute-start(bf16[256,2,1,64]{0,3,1,2:T(8,128)(2,1)S(1)} %collective-permute-done.2), channel_id=1, source_target_pairs={{0,4},{4,8},{8,12},{12,16},{16,20},{20,24},{24,28},{28,0},{1,5},{5... | collective-permute-start | bytes 196616 | tf_op jit(solution)/shard_map/ppermute | solution.py:68
  149.0 7.2 %collective-permute-start.4 = (bf16[256,2,1,64]{0,3,1,2:T(8,128)(2,1)S(1)}, bf16[256,2,1,64]{0,3,1,2:T(8,128)(2,1)S(1)}, u32[]{:S(2)}, u32[]{:S(2)}) collective-permute-start(bf16[256,2,1,64]{0,3,1,2:T(8,128)(2,1)S(1)} %collective-permute-done.3), channel_id=1, source_target_pairs={{0,4},{4,8},{8,12},{12,16},{16,20},{20,24},{24,28},{28,0},{1,5},{5... | collective-permute-start | bytes 196616 | tf_op jit(solution)/shard_map/ppermute | solution.py:68
  156.1 31.6 %collective-permute-start.5 = (bf16[256,2,1,64]{0,3,1,2:T(8,128)(2,1)S(1)}, bf16[256,2,1,64]{0,3,1,2:T(8,128)(2,1)S(1)}, u32[]{:S(2)}, u32[]{:S(2)}) collective-permute-start(bf16[256,2,1,64]{0,3,1,2:T(8,128)(2,1)S(1)} %collective-permute-done.4), channel_id=1, source_target_pairs={{0,4},{4,8},{8,12},{12,16},{16,20},{20,24},{24,28},{28,0},{1,5},{5... | collective-permute-start | bytes 196616 | tf_op jit(solution)/shard_map/ppermute | solution.py:68
  187.8 7.2 %collective-permute-start.6 = (bf16[256,2,1,64]{0,3,1,2:T(8,128)(2,1)S(1)}, bf16[256,2,1,64]{0,3,1,2:T(8,128)(2,1)S(1)}, u32[]{:S(2)}, u32[]{:S(2)}) collective-permute-start(bf16[256,2,1,64]{0,3,1,2:T(8,128)(2,1)S(1)} %collective-permute-done.5), channel_id=1, source_target_pairs={{0,4},{4,8},{8,12},{12,16},{16,20},{20,24},{24,28},{28,0},{1,5},{5... | collective-permute-start | bytes 196616 | tf_op jit(solution)/shard_map/ppermute | solution.py:68
  205.4 7.0 %copy-start.4 = (f32[128,2]{0,1:T(2,128)S(1)}, f32[128,2]{0,1:T(2,128)}, u32[]{:S(2)}) copy-start(f32[128,2]{0,1:T(2,128)} %param.24) | copy-start | bytes 3076
  208.8 31.2 %all-to-all-start.1 = ((bf16[8,48,2048]{2,1,0:T(8,128)(2,1)}), bf16[8,48,2048]{2,1,0:T(8,128)(2,1)S(1)}, u32[]{:S(2)}, u32[]{:S(2)}) async-start(bf16[8,48,2048]{2,1,0:T(8,128)(2,1)} %bitcast.149), calls=%async_computation.3 | async-start | bytes 3145728 | tf_op jit(solution)/shard_map/all_to_all | solution.py:152
Sparse Core Ops, SparseCore 0:
  56.8 45.3 all-gather.1
  120.4 58.8 reduce-scatter.4
  208.9 28.7 reduce-scatter.2
